TPU v7x, 32 devices: a whole 2x2x4 slice. The times are simulated.
32 devices in a mesh: grp: 2 (over y), sp: 4 (over z), tp: 4 (over x, core).
Axes of the slice: x: 2, y: 2, z: 4, core: 2. Of those that a mesh axis runs over, the one named last changes fastest.
Arguments:
- tokens: bfloat16 [6144, 2048], P(('grp', 'sp'), 'tp'), parts along dimension 0, may hold values from -8 to 8
- norm_gain: float32 [2, 2048], replicated, may hold values from 0.1 to 1.9
- w_value: bfloat16 [2, 2048, 2048], P(None, 'sp', 'tp'), may hold values from -0.125 to 0.125
- w_gate: bfloat16 [2, 2048, 2048], P(None, 'sp', 'tp'), may hold values from -0.125 to 0.125
- taps: float32 [2, 31, 2048], P(None, None, 'tp'), may hold values from -2 to 2
- ln_gain: float32 [2, 2048], P(None, 'tp'), may hold values from 0.1 to 1.9
- ln_shift: float32 [2, 2048], P(None, 'tp'), may hold values from -3 to 3
- w_out: bfloat16 [2, 2048, 2048], P(None, 'sp', 'tp'), may hold values from -0.125 to 0.125
Outputs:
- stream_out: bfloat16 [6144, 2048], P(('grp', 'sp'), 'tp'), parts along dimension 0
There are 2 independent parts, one for each index of `grp`. A program takes and returns all parts, laid end to end along the dimension named above; an argument that names none is the same for every part. Nothing has to cross between parts.
All inputs are finite; a program needn't handle non-finite values.
Results may differ from a plain program's by a relative error of at most 0.012.
Values may be sent and summed in bfloat16 or wider, within the bound.
A program may use at most 64 MiB of HBM per device.

v0:
```python
import functools

import jax
import jax.numpy as jnp
from jax import lax
from jax.experimental import pallas as pl
from jax.experimental.pallas import tpu as pltpu
from jax.sharding import PartitionSpec as P

MESH = pl.DeviceIdType.MESH
HALO = 16
LANES = 128
BLOCK = 64
LEAD = 4


def body(
    sizes,
    tokens,
    norm_gain,
    w_value,
    w_gate,
    taps_in,
    ln_gain,
    ln_shift,
    w_out,
    out,
    taps,
    weights,
    gathered,
    glu,
    conv,
    stats,
    load_sem,
    z_send,
    z_recv,
    y_send,
    y_recv,
    x_send,
    x_recv,
    s_send,
    s_recv,
    h_send,
    h_recv,
):
    groups, n, tp, chunks, subs, ahead = sizes
    chips = tp // 2
    grp, sp, me = lax.axis_index("grp"), lax.axis_index("sp"), lax.axis_index("tp")
    chip, core = me // 2, me % 2
    partner = chip * 2 + 1 - core
    layers, depth, cols = w_value.shape
    kernel = taps_in.shape[1]
    half = (kernel - 1) // 2
    count = tokens.shape[0]
    rows = count // chunks
    width = cols * tp
    pieces = layers * 3 * subs
    part = depth // (groups * subs)
    hops = n - 1
    per_matrix = subs * hops
    lead = LEAD
    f32, bf16 = jnp.float32, jnp.bfloat16

    def aligned(value, unit):
        return pl.multiple_of(value, unit)

    barrier = pltpu.get_barrier_semaphore()
    for off in range(1, tp):
        pl.semaphore_signal(
            barrier, inc=1, device_id={"tp": (me + off) % tp}, device_id_type=MESH
        )
    for off in range(1, groups):
        pl.semaphore_signal(
            barrier, inc=1, device_id={"grp": (grp + off) % groups}, device_id_type=MESH
        )

    @pl.when(sp > 0)
    def _():
        pl.semaphore_signal(barrier, inc=1, device_id={"sp": sp - 1}, device_id_type=MESH)

    @pl.when(sp < n - 1)
    def _():
        pl.semaphore_signal(barrier, inc=1, device_id={"sp": sp + 1}, device_id_type=MESH)

    def own_load(matrix):
        source = (w_value, w_gate, w_out)[matrix % 3]
        return pltpu.make_async_copy(
            source.at[matrix // 3],
            weights.at[matrix, pl.ds(aligned(sp * depth, 16), depth), :],
            load_sem.at[matrix],
        )

    taps_load = pltpu.make_async_copy(taps_in, taps, load_sem.at[layers * 3])
    for matrix in range(layers * 3):
        own_load(matrix).start()
    taps_load.start()

    def piece(block, m, quarter):
        start = block * depth + ((m % subs) * groups + quarter) * part
        return weights.at[m // subs, pl.ds(aligned(start, 16), part), :]

    def z_copy(way, m, hop, block):
        ref = piece(block, m, grp)
        return pltpu.make_async_remote_copy(
            src_ref=ref,
            dst_ref=ref,
            send_sem=z_send.at[way, m, hop],
            recv_sem=z_recv.at[way, m, hop],
            device_id={"sp": sp + 1 if way == 0 else sp - 1},
            device_id_type=MESH,
        )

    def y_copy(m, block, off, quarter):
        ref = piece(block, m, quarter)
        return pltpu.make_async_remote_copy(
            src_ref=ref,
            dst_ref=ref,
            send_sem=y_send.at[m, block, off - 1],
            recv_sem=y_recv.at[m, block, off - 1],
            device_id={"grp": (grp + off) % groups},
            device_id_type=MESH,
        )

    def send_own(m):
        @pl.when(sp < n - 1)
        def _():
            z_copy(0, m, 0, sp).start()

        @pl.when(sp > 0)
        def _():
            z_copy(1, m, 0, sp).start()

    def weight_step(k):
        m, r = k // hops, k % hops

        @pl.when(sp - (r + 1) >= 0)
        def _():
            block = sp - (r + 1)
            z_copy(0, m, r, block).wait_recv()

            @pl.when(sp < n - 1)
            def _():
                z_copy(0, m, r + 1, block).start()

            for off in range(1, groups):
                y_copy(m, block, off, grp).start()

        @pl.when(sp + (r + 1) < n)
        def _():
            block = sp + (r + 1)
            z_copy(1, m, r, block).wait_recv()

            @pl.when(sp > 0)
            def _():
                z_copy(1, m, r + 1, block).start()

            for off in range(1, groups):
                y_copy(m, block, off, grp).start()

        @pl.when(jnp.logical_and(r == hops - 1, m + ahead < pieces))
        def _():
            send_own(m + ahead)

    def weight_steps(low, high):
        lax.fori_loop(low, high, lambda k, c: (weight_step(k), c)[1], 0)

    def weight_share(low, high, i):
        span = high - low
        weight_steps(low + span * i // chunks, low + span * (i + 1) // chunks)

    def matrix_wait(matrix):
        def wait(i, c):
            m, block = matrix * subs + i // n, i % n

            @pl.when(block != sp)
            def _():
                for off in range(1, groups):
                    y_copy(m, block, off, (grp + groups - off) % groups).wait_recv()

            return c

        lax.fori_loop(0, subs * n, wait, 0)

    def chunk_rows(c):
        return pl.ds(aligned(c * rows, rows), rows)

    def x_copy(phase, c, source, slot, target):
        ref = gathered.at[phase, chunk_rows(c), pl.ds(aligned(source * cols, LANES), cols)]
        return pltpu.make_async_remote_copy(
            src_ref=ref,
            dst_ref=ref,
            send_sem=x_send.at[phase, c, slot],
            recv_sem=x_recv.at[phase, c, source],
            device_id={"tp": target},
            device_id_type=MESH,
        )

    def x_own(phase, c):
        for off in range(1, chips):
            x_copy(phase, c, me, off - 1, ((chip + off) % chips) * 2 + core).start()
        x_copy(phase, c, me, chips - 1, partner).start()

    def x_forward(phase, c):
        for off in range(1, chips):
            source = ((chip + off) % chips) * 2 + core
            x_copy(phase, c, source, 0, partner).wait_recv()
            x_copy(phase, c, source, chips - 1 + off, partner).start()

    def x_wait(phase, c):
        for off in range(chips):
            source = ((chip + off) % chips) * 2 + 1 - core
            x_copy(phase, c, source, 0, partner).wait_recv()

    def s_copy(phase, c, source, slot, target):
        ref = stats.at[phase, c, source]
        return pltpu.make_async_remote_copy(
            src_ref=ref,
            dst_ref=ref,
            send_sem=s_send.at[phase, c, slot],
            recv_sem=s_recv.at[phase, c, source],
            device_id={"tp": target},
            device_id_type=MESH,
        )

    def s_share(phase, c, first, second):
        lane = lax.broadcasted_iota(jnp.int32, (rows, LANES), 1)
        both = jnp.where(lane < 4, first, second)
        stats[phase, c, me] = both.T[:8]
        for off in range(1, tp):
            s_copy(phase, c, me, off - 1, (me + off) % tp).start()

    def s_total(phase, c):
        for off in range(1, tp):
            s_copy(phase, c, (me + off) % tp, 0, me).wait_recv()
        total = stats[phase, c, 0]
        for source in range(1, tp):
            total = total + stats[phase, c, source]
        return jnp.concatenate([total] * (LANES // 8), axis=0).T

    def h_copy(layer, way):
        if way == 0:
            source, target, device = count, 0, sp + 1
        else:
            source, target, device = HALO, HALO + count, sp - 1
        return pltpu.make_async_remote_copy(
            src_ref=glu.at[layer, pl.ds(source, HALO), :],
            dst_ref=glu.at[layer, pl.ds(target, HALO), :],
            send_sem=h_send.at[layer, way],
            recv_sem=h_recv.at[layer, way],
            device_id={"sp": device},
            device_id_type=MESH,
        )

    mine = pl.ds(aligned(me * cols, LANES), cols)

    def share_stream(layer, c, wide):
        s_share(2 * layer, c, jnp.sum(wide * wide, axis=1, keepdims=True), 0.0)
        gain = norm_gain[pl.ds(layer, 1), mine]
        gathered[2 * layer, chunk_rows(c), mine] = (wide * gain).astype(bf16)
        x_own(2 * layer, c)

    def loop(function):
        lax.fori_loop(0, chunks, lambda i, c: (function(i), c)[1], 0)

    def inner_first(i):
        return (1 + 2 * i) % chunks

    def ends_first(i):
        return (2 * i) % chunks

    for layer in range(layers):

        @pl.when(sp == 0)
        def _():
            glu[layer, pl.ds(0, HALO), :] = jnp.zeros((HALO, cols), bf16)

        @pl.when(sp == n - 1)
        def _():
            glu[layer, pl.ds(HALO + count, HALO), :] = jnp.zeros((HALO, cols), bf16)

    for matrix in range(layers * 3):
        own_load(matrix).wait()
    taps_load.wait()
    pl.semaphore_wait(
        barrier,
        tp - 1 + groups - 1 + (sp > 0).astype(jnp.int32) + (sp < n - 1).astype(jnp.int32),
    )
    for m in range(ahead):
        send_own(m)

    loop(lambda c: share_stream(0, c, tokens[chunk_rows(c), :].astype(f32)))

    def gated(layer, low, high, i):
        c = ends_first(i)
        phase = 2 * layer
        scale = lax.rsqrt(s_total(phase, c)[:, :1] / width + 1e-06)
        block = gathered[phase, chunk_rows(c), :]
        value = jnp.dot(block, weights[3 * layer], preferred_element_type=f32) * scale
        gate = jnp.dot(block, weights[3 * layer + 1], preferred_element_type=f32) * scale
        glu[layer, pl.ds(aligned(HALO + c * rows, HALO), rows), :] = (
            value * jax.nn.sigmoid(gate)
        ).astype(bf16)

        @pl.when(jnp.logical_and(c == 0, sp > 0))
        def _():
            h_copy(layer, 1).start()

        @pl.when(jnp.logical_and(c == chunks - 1, sp < n - 1))
        def _():
            h_copy(layer, 0).start()

        weight_share(low, high, i)

    shift = HALO - half
    groups_of_8 = (kernel + shift + 7) // 8
    window = BLOCK + 8 * groups_of_8

    def convolve(layer, c):
        lane_blocks = cols // LANES

        def block(i, carry):
            base = aligned(c * rows + (i // lane_blocks) * BLOCK, BLOCK)
            lanes = pl.ds(aligned((i % lane_blocks) * LANES, LANES), LANES)
            values = glu[layer, pl.ds(base, window), lanes].astype(f32)
            total = None
            for j in range(8):
                partial = None
                for g in range(groups_of_8):
                    tap = 8 * g + j - shift
                    if tap < 0 or tap >= kernel:
                        continue
                    term = taps[layer, pl.ds(tap, 1), lanes] * values[8 * g : 8 * g + BLOCK + 8]
                    partial = term if partial is None else partial + term
                piece_j = partial[j : j + BLOCK]
                total = piece_j if total is None else total + piece_j
            conv[pl.ds(base, BLOCK), lanes] = total
            return carry

        lax.fori_loop(0, rows // BLOCK * lane_blocks, block, 0)

    def mixed(layer, low, high, i):
        c = inner_first(i)

        @pl.when(jnp.logical_and(c == 0, sp > 0))
        def _():
            h_copy(layer, 0).wait_recv()

        @pl.when(jnp.logical_and(c == chunks - 1, sp < n - 1))
        def _():
            h_copy(layer, 1).wait_recv()

        convolve(layer, c)
        whole = conv[chunk_rows(c), :]
        s_share(
            2 * layer + 1,
            c,
            jnp.sum(whole, axis=1, keepdims=True),
            jnp.sum(whole * whole, axis=1, keepdims=True),
        )
        weight_share(low, high, i)

    def activate(layer, i):
        c = inner_first(i)
        total = s_total(2 * layer + 1, c)
        mean = total[:, :1] / width
        var = total[:, 4:5] / width - mean * mean
        gain = ln_gain[pl.ds(layer, 1), :]
        moved = ln_shift[pl.ds(layer, 1), :]
        shaped = (conv[chunk_rows(c), :] - mean) * lax.rsqrt(var + 1e-05) * gain + moved
        act = shaped * jax.nn.sigmoid(shaped)
        gathered[2 * layer + 1, chunk_rows(c), mine] = act.astype(bf16)
        x_own(2 * layer + 1, c)

    def close(layer, low, high, i):
        c = inner_first(i)
        phase = 2 * layer + 1
        x_forward(phase, c)
        x_wait(phase, c)
        update = jnp.dot(
            gathered[phase, chunk_rows(c), :],
            weights[3 * layer + 2],
            preferred_element_type=f32,
        )
        source = tokens if layer == 0 else out
        stream = (source[chunk_rows(c), :].astype(f32) + update).astype(bf16)
        out[chunk_rows(c), :] = stream
        if layer + 1 < layers:
            share_stream(layer + 1, c, stream.astype(f32))
            weight_share(low, high, i)

    def arrive(layer, low, high, i):
        c = i if layer == 0 else inner_first(i)
        x_forward(2 * layer, c)
        x_wait(2 * layer, c)
        weight_share(low, high, i)

    def due(k):
        return min(k + lead, pieces * hops)

    for layer in range(layers):
        first = 3 * layer * per_matrix
        closing = first + 2 * per_matrix
        early = due(closing + per_matrix // 6)
        middle = due(closing + per_matrix // 2)
        after = due(closing + per_matrix)
        closing = due(closing)
        opening = 0 if layer == 0 else due(first + per_matrix)
        loop(functools.partial(arrive, layer, opening, closing))
        matrix_wait(3 * layer)
        matrix_wait(3 * layer + 1)
        loop(functools.partial(gated, layer, closing, early))
        loop(functools.partial(mixed, layer, early, middle))
        loop(functools.partial(activate, layer))
        weight_steps(middle, after)
        matrix_wait(3 * layer + 2)
        loop(functools.partial(close, layer, after, due(first + 4 * per_matrix)))

    def drain_weights(i, carry):
        m, block = i // n, i % n

        @pl.when(block <= sp)
        def _():
            @pl.when(sp < n - 1)
            def _():
                z_copy(0, m, sp - block, block).wait_send()

        @pl.when(block >= sp)
        def _():
            @pl.when(sp > 0)
            def _():
                z_copy(1, m, block - sp, block).wait_send()

        @pl.when(block != sp)
        def _():
            for off in range(1, groups):
                y_copy(m, block, off, grp).wait_send()

        return carry

    lax.fori_loop(0, pieces * n, drain_weights, 0)

    def drain_chunks(i, carry):
        phase, c = i // chunks, i % chunks
        for slot in range(tp - 1):
            x_copy(phase, c, me, slot, partner).wait_send()
            s_copy(phase, c, me, slot, partner).wait_send()
        return carry

    lax.fori_loop(0, 2 * layers * chunks, drain_chunks, 0)
    for layer in range(layers):

        @pl.when(sp < n - 1)
        def _():
            h_copy(layer, 0).wait_send()

        @pl.when(sp > 0)
        def _():
            h_copy(layer, 1).wait_send()


def solution(mesh):
    groups, n, tp = mesh.shape["grp"], mesh.shape["sp"], mesh.shape["tp"]

    def shards(tokens, norm_gain, w_value, w_gate, taps, ln_gain, ln_shift, w_out):
        layers, depth, cols = w_value.shape
        count = tokens.shape[0]
        chunks = 3
        subs = 2 if depth >= 512 else 1
        ahead = 2
        pieces = layers * 3 * subs
        rows = count // chunks
        vmem = pl.BlockSpec(memory_space=pltpu.VMEM)
        hbm = pl.BlockSpec(memory_space=pl.ANY)
        dma = pltpu.SemaphoreType.DMA
        return pl.pallas_call(
            functools.partial(body, (groups, n, tp, chunks, subs, ahead)),
            out_shape=jax.ShapeDtypeStruct((count, cols), jnp.bfloat16),
            in_specs=[vmem, vmem, hbm, hbm, hbm, vmem, vmem, hbm],
            out_specs=vmem,
            scratch_shapes=[
                pltpu.VMEM(taps.shape, jnp.float32),
                pltpu.VMEM((layers * 3, depth * n, cols), jnp.bfloat16),
                pltpu.VMEM((2 * layers, count, cols * tp), jnp.bfloat16),
                pltpu.VMEM((layers, count + 2 * HALO, cols), jnp.bfloat16),
                pltpu.VMEM((count, cols), jnp.float32),
                pltpu.VMEM((2 * layers, chunks, tp, 8, rows), jnp.float32),
                dma((layers * 3 + 1,)),
                dma((2, pieces, n - 1)),
                dma((2, pieces, n - 1)),
                dma((pieces, n, groups - 1)),
                dma((pieces, n, groups - 1)),
                dma((2 * layers, chunks, tp - 1)),
                dma((2 * layers, chunks, tp)),
                dma((2 * layers, chunks, tp - 1)),
                dma((2 * layers, chunks, tp)),
                dma((layers, 2)),
                dma((layers, 2)),
            ],
            compiler_params=pltpu.CompilerParams(
                collective_id=0, has_side_effects=True, vmem_limit_bytes=60 * 1024 * 1024
            ),
        )(tokens, norm_gain, w_value, w_gate, taps, ln_gain, ln_shift, w_out)

    return jax.shard_map(
        shards,
        mesh=mesh,
        in_specs=(
            P(("grp", "sp"), "tp"),
            P(),
            P(None, "sp", "tp"),
            P(None, "sp", "tp"),
            P(None, None, "tp"),
            P(None, "tp"),
            P(None, "tp"),
            P(None, "sp", "tp"),
        ),
        out_specs=P(("grp", "sp"), "tp"),
        check_vma=False,
    )
```

profile of v0, /device:TPU:1, one launch (start us, length us, event | category | flops | bytes accessed | tf_op | source)
XLA Modules:
  0.0 150.1 jit_solution(10590572883804128225)
XLA Ops:
  0.0 1.6 %copy.9.taps_in = f32[2,31,512]{2,1,0:T(8,128)} copy(f32[2,31,512]{2,0,1:T(2,128)} %param.12) | data formatting | bytes 253952 | tf_op args[4]
  1.6 146.4 %shard_map.82 = bf16[768,512]{1,0:T(8,128)(2,1)} custom-call(bf16[768,512]{1,0:T(8,128)(2,1)} %tokens.1, f32[2,2048]{1,0:T(2,128)} %norm_gain.1, bf16[2,512,512]{2,1,0:T(8,128)(2,1)} %w_value.1, bf16[2,512,512]{2,1,0:T(8,128)(2,1)} %w_gate.1, f32[2,31,512]{2,1,0:T(8,128)} %copy.9.taps_in, f32[2,512]{1,0:T(2,128)} %ln_gain.1, f32[2,512]{1,0:T(2,128)} %ln_shift.1, ...), custom_call_target="tpu_custom_call" | custom-call | tf_op jit(solution)/shard_map/pallas_call | solution.py:475
  148.0 2.1 %copy.11 = bf16[768,512]{1,0:T(8,128)(2,1)} copy(bf16[768,512]{1,0:T(8,128)(2,1)} %shard_map.82) | data formatting | bytes 1572864
where the time goes:
time: 150 us
  Pallas kernels  146 us (97%)
  local copies, waits for them, and re-layouts  3.65 us (2%)
    pallas_call x1, Pallas kernels, shards(): pl.pallas_call(functools.partial(body, (groups, n, tp, chunks, subs, ahea...  146 us
    unnamed x2, local copies, waits for them, and re-layouts  3.65 us

commit v1 on v0

v1 whole, which is shorter than its diff:
```python
import functools

import jax
import jax.numpy as jnp
from jax import lax
from jax.experimental import pallas as pl
from jax.experimental.pallas import tpu as pltpu
from jax.sharding import PartitionSpec as P

MESH = pl.DeviceIdType.MESH
HALO = 16
LANES = 128
BLOCK = 64


def body(
    sizes,
    tokens,
    norm_gain,
    w_value,
    w_gate,
    taps_in,
    ln_gain,
    ln_shift,
    w_out,
    out,
    taps,
    weights,
    gathered,
    glu,
    conv,
    act,
    sums,
    stats,
    norms,
    load_sem,
    z_send,
    z_recv,
    y_send,
    y_recv,
    x_send,
    x_recv,
    s_send,
    s_recv,
    h_send,
    h_recv,
    n_send,
    n_recv,
):
    groups, n, tp, chunks, subs = sizes
    chips = tp // 2
    grp, sp, me = lax.axis_index("grp"), lax.axis_index("sp"), lax.axis_index("tp")
    chip, core = me // 2, me % 2
    partner = chip * 2 + 1 - core
    layers, depth, cols = w_value.shape
    kernel = taps_in.shape[0]
    half = (kernel - 1) // 2
    count = tokens.shape[0]
    rows = count // chunks
    width = cols * tp
    hops = n - 1
    f32, bf16 = jnp.float32, jnp.bfloat16

    def aligned(value, unit):
        return pl.multiple_of(value, unit)

    barrier = pltpu.get_barrier_semaphore()
    for off in range(1, tp):
        pl.semaphore_signal(
            barrier, inc=1, device_id={"tp": (me + off) % tp}, device_id_type=MESH
        )
    for off in range(1, groups):
        pl.semaphore_signal(
            barrier, inc=1, device_id={"grp": (grp + off) % groups}, device_id_type=MESH
        )

    @pl.when(sp > 0)
    def _():
        pl.semaphore_signal(barrier, inc=1, device_id={"sp": sp - 1}, device_id_type=MESH)

    @pl.when(sp < n - 1)
    def _():
        pl.semaphore_signal(barrier, inc=1, device_id={"sp": sp + 1}, device_id_type=MESH)

    qc = cols // subs
    total = layers * 3 * subs
    part = depth // groups
    span = 2 * hops

    def own_load(m):
        layer, j = m // (3 * subs), m % (3 * subs)
        if j < 2 * subs:
            source, q = (w_value, w_gate)[j % 2], j // 2
        else:
            source, q = w_out, j - 2 * subs
        return pltpu.make_async_copy(
            source.at[layer, :, pl.ds(q * qc, qc)],
            weights.at[m, pl.ds(aligned(sp * depth, 16), depth), :],
            load_sem.at[m],
        )

    taps_load = pltpu.make_async_copy(taps_in, taps, load_sem.at[total])
    for m in range(total):
        own_load(m).start()
    taps_load.start()

    def piece(block, m, quarter):
        return weights.at[m, pl.ds(aligned(block * depth + quarter * part, 16), part), :]

    def z_copy(way, m, hop, block):
        ref = piece(block, m, grp)
        return pltpu.make_async_remote_copy(
            src_ref=ref,
            dst_ref=ref,
            send_sem=z_send.at[way, m, hop],
            recv_sem=z_recv.at[way, m, hop],
            device_id={"sp": sp + 1 if way == 0 else sp - 1},
            device_id_type=MESH,
        )

    def y_copy(m, block, off, quarter):
        ref = piece(block, m, quarter)
        return pltpu.make_async_remote_copy(
            src_ref=ref,
            dst_ref=ref,
            send_sem=y_send.at[m, block, off - 1],
            recv_sem=y_recv.at[m, block, off - 1],
            device_id={"grp": (grp + off) % groups},
            device_id_type=MESH,
        )

    last_up = jnp.maximum(sp - 1, 0)
    last_down = jnp.maximum(n - 2 - sp, 0)

    def weight_step(k):
        m, r, p = 2 * (k // span) + k % 2, (k % span) // 2, k % 2

        @pl.when(sp - (r + 1) >= 0)
        def _():
            block = sp - (r + 1)
            z_copy(0, m, r, block).wait_recv()

            @pl.when(sp < n - 1)
            def _():
                z_copy(0, m, r + 1, block).start()

            for off in range(1, groups):
                y_copy(m, block, off, grp).start()

        @pl.when(sp + (r + 1) < n)
        def _():
            block = sp + (r + 1)
            z_copy(1, m, r, block).wait_recv()

            @pl.when(sp > 0)
            def _():
                z_copy(1, m, r + 1, block).start()

            for off in range(1, groups):
                y_copy(m, block, off, grp).start()

        more = jnp.logical_and(p == 1, m + 2 < total)

        @pl.when(jnp.logical_and(r == last_up, jnp.logical_and(more, sp < n - 1)))
        def _():
            z_copy(0, m + 1, 0, sp).start()
            z_copy(0, m + 2, 0, sp).start()

        @pl.when(jnp.logical_and(r == last_down, jnp.logical_and(more, sp > 0)))
        def _():
            z_copy(1, m + 1, 0, sp).start()
            z_copy(1, m + 2, 0, sp).start()


    def weight_steps(low, high):
        lax.fori_loop(low, high, lambda k, c: (weight_step(k), c)[1], 0)

    def weight_wait(m):
        def wait(block, c):
            @pl.when(block != sp)
            def _():
                for off in range(1, groups):
                    y_copy(m, block, off, (grp + groups - off) % groups).wait_recv()

            return c

        lax.fori_loop(0, n, wait, 0)

    def chunk_rows(c):
        return pl.ds(aligned(c * rows, rows), rows)

    def x_copy(phase, c, source, slot, target):
        layer, sub = phase // (1 + subs), phase % (1 + subs)
        if sub == 0:
            lanes = pl.ds(aligned(source * cols, LANES), cols)
        else:
            lanes = pl.ds(aligned(source * cols + (sub - 1) * qc, LANES), qc)
        ref = gathered.at[2 * layer + min(sub, 1), chunk_rows(c), lanes]
        return pltpu.make_async_remote_copy(
            src_ref=ref,
            dst_ref=ref,
            send_sem=x_send.at[phase, c, slot],
            recv_sem=x_recv.at[phase, c, source],
            device_id={"tp": target},
            device_id_type=MESH,
        )

    def x_own(phase, c):
        for off in range(1, chips):
            x_copy(phase, c, me, off - 1, ((chip + off) % chips) * 2 + core).start()
        x_copy(phase, c, me, chips - 1, partner).start()

    def x_forward(phase, c):
        for off in range(1, chips):
            source = ((chip + off) % chips) * 2 + core
            x_copy(phase, c, source, 0, partner).wait_recv()
            x_copy(phase, c, source, chips - 1 + off, partner).start()

    def x_wait(phase, c):
        for off in range(chips):
            source = ((chip + off) % chips) * 2 + 1 - core
            x_copy(phase, c, source, 0, partner).wait_recv()

    def s_copy(phase, c, source, slot, target):
        ref = stats.at[phase, c, source]
        return pltpu.make_async_remote_copy(
            src_ref=ref,
            dst_ref=ref,
            send_sem=s_send.at[phase, c, slot],
            recv_sem=s_recv.at[phase, c, source],
            device_id={"tp": target},
            device_id_type=MESH,
        )

    def s_share(phase, c, values):
        stats[phase, c, me] = values.T[:8]
        for off in range(1, tp):
            s_copy(phase, c, me, off - 1, (me + off) % tp).start()

    def s_wait(phase, c):
        for off in range(1, tp):
            s_copy(phase, c, (me + off) % tp, 0, me).wait_recv()

    def s_total(phase, c):
        total = stats[phase, c, 0]
        for source in range(1, tp):
            total = total + stats[phase, c, source]
        return total

    def columns(rows_of_8):
        block = jnp.concatenate(rows_of_8, axis=0)
        return jnp.concatenate([block] * (LANES // block.shape[0]), axis=0).T

    def n_copy(which, source, slot, target):
        return pltpu.make_async_remote_copy(
            src_ref=(ln_gain, ln_shift)[which],
            dst_ref=norms.at[which, source],
            send_sem=n_send.at[which, slot],
            recv_sem=n_recv.at[which, source],
            device_id={"tp": target},
            device_id_type=MESH,
        )

    def h_copy(layer, q, way):
        if way == 0:
            source, target, device = count, 0, sp + 1
        else:
            source, target, device = HALO, HALO + count, sp - 1
        lanes = pl.ds(q * qc, qc)
        return pltpu.make_async_remote_copy(
            src_ref=glu.at[layer, pl.ds(source, HALO), lanes],
            dst_ref=glu.at[layer, pl.ds(target, HALO), lanes],
            send_sem=h_send.at[layer, q, way],
            recv_sem=h_recv.at[layer, q, way],
            device_id={"sp": device},
            device_id_type=MESH,
        )

    mine = pl.ds(aligned(me * cols, LANES), cols)
    lane = lax.broadcasted_iota(jnp.int32, (rows, LANES), 1)

    def share_stream(layer, c, wide):
        gain = norm_gain[pl.ds(layer, 1), mine]
        gathered[2 * layer, chunk_rows(c), mine] = (wide * gain).astype(bf16)
        x_own(layer * (1 + subs), c)
        square = jnp.sum(wide * wide, axis=1, keepdims=True)
        s_share(2 * layer, c, jnp.where(lane == 0, square, 0.0))

    def loop(function):
        lax.fori_loop(0, chunks, lambda i, c: (function(i), c)[1], 0)

    def inner_first(i):
        return (1 + 2 * i) % chunks

    def ends_first(i):
        return (2 * i) % chunks

    for layer in range(layers):

        @pl.when(sp == 0)
        def _():
            glu[layer, pl.ds(0, HALO), :] = jnp.zeros((HALO, cols), bf16)

        @pl.when(sp == n - 1)
        def _():
            glu[layer, pl.ds(HALO + count, HALO), :] = jnp.zeros((HALO, cols), bf16)

    for m in range(2):
        own_load(m).wait()
    pl.semaphore_wait(
        barrier,
        tp - 1 + groups - 1 + (sp > 0).astype(jnp.int32) + (sp < n - 1).astype(jnp.int32),
    )
    for m in range(2):

        @pl.when(sp < n - 1)
        def _():
            z_copy(0, m, 0, sp).start()

        @pl.when(sp > 0)
        def _():
            z_copy(1, m, 0, sp).start()

    loop(lambda c: share_stream(0, c, tokens[chunk_rows(c), :].astype(f32)))
    for which in range(2):
        for off in range(1, tp):
            n_copy(which, me, off - 1, (me + off) % tp).start()
    norms[0, me] = ln_gain[...]
    norms[1, me] = ln_shift[...]
    for m in range(2, total):
        own_load(m).wait()
    taps_load.wait()

    done = [0]

    def share(goal):
        low = done[0]
        high = max(low, min(goal, total * hops))
        done[0] = high
        return lambda i: weight_steps(
            low + (high - low) * i // chunks, low + (high - low) * (i + 1) // chunks
        )

    def advance(goal):
        low = done[0]
        high = max(low, min(goal, total * hops))
        done[0] = high
        weight_steps(low, high)

    def gated(layer, q, steps, i):
        c = ends_first(i)
        if q == 0:
            s_wait(2 * layer, c)
        scale = lax.rsqrt(columns([s_total(2 * layer, c)])[:, :1] / width + 1e-06)
        block = gathered[2 * layer, chunk_rows(c), :]
        first = layer * 3 * subs + 2 * q
        value = jnp.dot(block, weights[first], preferred_element_type=f32) * scale
        gate = jnp.dot(block, weights[first + 1], preferred_element_type=f32) * (0.5 * scale)
        glu[layer, pl.ds(aligned(HALO + c * rows, HALO), rows), pl.ds(q * qc, qc)] = (
            value * (0.5 + 0.5 * jnp.tanh(gate))
        ).astype(bf16)

        @pl.when(jnp.logical_and(c == 0, sp > 0))
        def _():
            h_copy(layer, q, 1).start()

        @pl.when(jnp.logical_and(c == chunks - 1, sp < n - 1))
        def _():
            h_copy(layer, q, 0).start()

        steps(i)

    shift = HALO - half
    groups_of_8 = (kernel + shift + 7) // 8
    window = BLOCK + 8 * groups_of_8

    def convolve(layer, q, c):
        lane_blocks = qc // LANES

        def block(i, carry):
            base = aligned(c * rows + (i // lane_blocks) * BLOCK, BLOCK)
            inside = aligned((i % lane_blocks) * LANES, LANES)
            lanes = pl.ds(aligned(q * qc + inside, LANES), LANES)
            values = glu[layer, pl.ds(base, window), lanes].astype(f32)
            total = None
            for j in range(8):
                partial = None
                for g in range(groups_of_8):
                    tap = 8 * g + j - shift
                    if tap < 0 or tap >= kernel:
                        continue
                    term = taps[tap, pl.ds(layer, 1), lanes] * values[8 * g : 8 * g + BLOCK + 8]
                    partial = term if partial is None else partial + term
                piece_j = partial[j : j + BLOCK]
                total = piece_j if total is None else total + piece_j
            conv[pl.ds(base, BLOCK), pl.ds(inside, LANES)] = total
            return carry

        lax.fori_loop(0, rows // BLOCK * lane_blocks, block, 0)

    def mixed(layer, q, steps, i):
        c = inner_first(i)

        @pl.when(jnp.logical_and(c == 0, sp > 0))
        def _():
            h_copy(layer, q, 0).wait_recv()

        @pl.when(jnp.logical_and(c == chunks - 1, sp < n - 1))
        def _():
            h_copy(layer, q, 1).wait_recv()

        convolve(layer, q, c)
        whole = conv[chunk_rows(c), :]
        row_sum = jnp.sum(whole, axis=1, keepdims=True)
        lanes = pl.ds(aligned(me * cols + q * qc, LANES), qc)
        gathered[2 * layer + 1, chunk_rows(c), lanes] = (whole - row_sum / qc).astype(bf16)
        x_own(layer * (1 + subs) + 1 + q, c)
        square = jnp.sum(whole * whole, axis=1, keepdims=True)
        both = jnp.where(lane == q, row_sum, jnp.where(lane == 4, square, 0.0))
        if q > 0:
            both = both + sums[chunk_rows(c), :]
        if q < subs - 1:
            sums[chunk_rows(c), :] = both
        else:
            s_share(2 * layer + 1, c, both)
        steps(i)

    def arrive(phase, steps, i):
        c = i if phase == 0 else inner_first(i)
        steps(i)
        x_forward(phase, c)
        x_wait(phase, c)

    sublane = lax.broadcasted_iota(jnp.int32, (8, rows), 0)

    def activate(layer, steps, i):
        c = inner_first(i)
        phase = 2 * layer + 1
        x_forward(layer * (1 + subs) + subs, c)
        x_wait(layer * (1 + subs) + subs, c)
        s_wait(phase, c)
        total = s_total(phase, c)
        mean = total[0:1]
        for q in range(1, subs):
            mean = mean + total[q : q + 1]
        mean = mean / width
        inverse = lax.rsqrt(total[4:5] / width - mean * mean + 1e-05)
        offsets = [
            jnp.where(sublane == 4, inverse, (stats[phase, c, source] / qc - mean) * inverse)
            for source in range(tp)
        ]
        table = columns(offsets)
        for source in range(tp):
            for q in range(subs):
                lanes = pl.ds(source * cols + q * qc, qc)
                inside = pl.ds(q * qc, qc)
                gain = 0.5 * norms[0, source, pl.ds(layer, 1), inside]
                moved = 0.5 * norms[1, source, pl.ds(layer, 1), inside]
                offset = table[:, 8 * source + q : 8 * source + q + 1]
                block = gathered[phase, chunk_rows(c), lanes].astype(f32)
                shaped = (block * table[:, 4:5] + offset) * gain + moved
                act[chunk_rows(c), lanes] = (shaped + shaped * jnp.tanh(shaped)).astype(bf16)
        steps(i)

    def close(layer, q, steps, i):
        c = inner_first(i)
        update = jnp.dot(
            act[chunk_rows(c), :],
            weights[layer * 3 * subs + 2 * subs + q],
            preferred_element_type=f32,
        )
        source = tokens if layer == 0 else out
        lanes = pl.ds(q * qc, qc)
        out[chunk_rows(c), lanes] = (source[chunk_rows(c), lanes].astype(f32) + update).astype(bf16)
        if q == subs - 1 and layer + 1 < layers:
            share_stream(layer + 1, c, out[chunk_rows(c), :].astype(f32))
        steps(i)

    def need(m):
        return (m // 2 + 1) * span

    def part_of(steps):
        return steps * span // 6

    for layer in range(layers):
        first = layer * 3 * subs
        loop(functools.partial(arrive, layer * (1 + subs), share(done[0] + part_of(6))))
        if layer == 0:
            for which in range(2):
                for off in range(1, tp):
                    n_copy(which, (me + off) % tp, 0, me).wait_recv()
        for q in range(subs):
            advance(need(first + 2 * q + 1) + part_of(2))
            weight_wait(first + 2 * q)
            weight_wait(first + 2 * q + 1)
            loop(functools.partial(gated, layer, q, share(done[0] + part_of(1))))
            loop(functools.partial(mixed, layer, q, share(done[0] + part_of(1))))
            if q < subs - 1:
                loop(functools.partial(arrive, layer * (1 + subs) + 1 + q, share(done[0] + part_of(3))))
        last = first + 2 * subs
        advance(need(last + subs - 1) + 0)
        loop(functools.partial(activate, layer, share(done[0] + 0)))
        advance(need(last + subs - 1) + part_of(2))
        for q in range(subs):
            weight_wait(last + q)
            loop(functools.partial(close, layer, q, share(done[0])))
    advance(total * hops)

    def drain_weights(i, carry):
        m, block = i // n, i % n

        @pl.when(block <= sp)
        def _():
            @pl.when(sp < n - 1)
            def _():
                z_copy(0, m, sp - block, block).wait_send()

        @pl.when(block >= sp)
        def _():
            @pl.when(sp > 0)
            def _():
                z_copy(1, m, block - sp, block).wait_send()

        @pl.when(block != sp)
        def _():
            for off in range(1, groups):
                y_copy(m, block, off, grp).wait_send()

        return carry

    lax.fori_loop(0, total * n, drain_weights, 0)

    def drain_chunks(c, carry):
        for slot in range(tp - 1):
            for phase in range(layers * (1 + subs)):
                x_copy(phase, c, me, slot, partner).wait_send()
            for phase in range(2 * layers):
                s_copy(phase, c, me, slot, partner).wait_send()
        return carry

    lax.fori_loop(0, chunks, drain_chunks, 0)
    for which in range(2):
        for slot in range(tp - 1):
            n_copy(which, me, slot, partner).wait_send()
    for layer in range(layers):
        for q in range(subs):

            @pl.when(sp < n - 1)
            def _():
                h_copy(layer, q, 0).wait_send()

            @pl.when(sp > 0)
            def _():
                h_copy(layer, q, 1).wait_send()


def solution(mesh):
    groups, n, tp = mesh.shape["grp"], mesh.shape["sp"], mesh.shape["tp"]

    def shards(tokens, norm_gain, w_value, w_gate, taps, ln_gain, ln_shift, w_out):
        layers, depth, cols = w_value.shape
        count = tokens.shape[0]
        chunks = 3
        subs = 2 if cols % (2 * LANES) == 0 else 1
        pieces = layers * 3 * subs
        taps = jnp.transpose(taps, (1, 0, 2))
        rows = count // chunks
        vmem = pl.BlockSpec(memory_space=pltpu.VMEM)
        hbm = pl.BlockSpec(memory_space=pl.ANY)
        dma = pltpu.SemaphoreType.DMA
        return pl.pallas_call(
            functools.partial(body, (groups, n, tp, chunks, subs)),
            out_shape=jax.ShapeDtypeStruct((count, cols), jnp.bfloat16),
            in_specs=[vmem, vmem, hbm, hbm, hbm, vmem, vmem, hbm],
            out_specs=vmem,
            scratch_shapes=[
                pltpu.VMEM(taps.shape, jnp.float32),
                pltpu.VMEM((pieces, depth * n, cols // subs), jnp.bfloat16),
                pltpu.VMEM((2 * layers, count, cols * tp), jnp.bfloat16),
                pltpu.VMEM((layers, count + 2 * HALO, cols), jnp.bfloat16),
                pltpu.VMEM((count, cols // subs), jnp.float32),
                pltpu.VMEM((count, cols * tp), jnp.bfloat16),
                pltpu.VMEM((count, LANES), jnp.float32),
                pltpu.VMEM((2 * layers, chunks, tp, 8, rows), jnp.float32),
                pltpu.VMEM((2, tp, layers, cols), jnp.float32),
                dma((pieces + 1,)),
                dma((2, pieces, n - 1)),
                dma((2, pieces, n - 1)),
                dma((pieces, n, groups - 1)),
                dma((pieces, n, groups - 1)),
                dma((layers * (1 + subs), chunks, tp - 1)),
                dma((layers * (1 + subs), chunks, tp)),
                dma((2 * layers, chunks, tp - 1)),
                dma((2 * layers, chunks, tp)),
                dma((layers, subs, 2)),
                dma((layers, subs, 2)),
                dma((2, tp - 1)),
                dma((2, tp)),
            ],
            compiler_params=pltpu.CompilerParams(
                collective_id=0, has_side_effects=True, vmem_limit_bytes=60 * 1024 * 1024
            ),
        )(tokens, norm_gain, w_value, w_gate, taps, ln_gain, ln_shift, w_out)

    return jax.shard_map(
        shards,
        mesh=mesh,
        in_specs=(
            P(("grp", "sp"), "tp"),
            P(),
            P(None, "sp", "tp"),
            P(None, "sp", "tp"),
            P(None, None, "tp"),
            P(None, "tp"),
            P(None, "tp"),
            P(None, "sp", "tp"),
        ),
        out_specs=P(("grp", "sp"), "tp"),
        check_vma=False,
    )
```

time: 150 us -> 138 us (0.920)
  Pallas kernels: 146 us -> 136 us
  local copies, waits for them, and re-layouts: 3.65 us -> 2.06 us
    pallas_call x1, Pallas kernels: 146 us -> 136 us  [shards(): pl.pallas_call(functools.partial(body, (groups, n, tp, chunks, subs)), ou...]
    unnamed x2 -> x1, local copies, waits for them, and re-layouts: 3.65 us -> 2.06 us
where the time goes in v1:
time: 138 us
  Pallas kernels  136 us (99%)
  local copies, waits for them, and re-layouts  2.06 us (1%)
    pallas_call x1, Pallas kernels, shards(): pl.pallas_call(functools.partial(body, (groups, n, tp, chunks, subs)), ou...  136 us

profile of v1, /device:TPU:1, one launch (start us, length us, event | category | flops | bytes accessed | tf_op | source)
XLA Modules:
  0.0 138.0 jit_solution(4685149534498796475)
XLA Ops:
  0.0 136.0 %shard_map.82 = bf16[768,512]{1,0:T(8,128)(2,1)} custom-call(bf16[768,512]{1,0:T(8,128)(2,1)} %tokens.1, f32[2,2048]{1,0:T(2,128)} %norm_gain.1, bf16[2,512,512]{2,1,0:T(8,128)(2,1)} %w_value.1, bf16[2,512,512]{2,1,0:T(8,128)(2,1)} %w_gate.1, f32[31,2,512]{2,1,0:T(2,128)} %bitcast.1, f32[2,512]{1,0:T(2,128)} %ln_gain.1, f32[2,512]{1,0:T(2,128)} %ln_shift.1, ...), custom_call_target="tpu_custom_call" | custom-call | tf_op jit(solution)/shard_map/pallas_call | solution.py:571
  136.0 2.1 %copy.10 = bf16[768,512]{1,0:T(8,128)(2,1)} copy(bf16[768,512]{1,0:T(8,128)(2,1)} %shard_map.82) | data formatting | bytes 1572864

commit v2 on v1

--- a/solution.py
+++ b/solution.py
@@ -15,8 +15,8 @@
 
 def body(
     sizes,
-    tokens,
-    norm_gain,
+    tokens_in,
+    gain_in,
     w_value,
     w_gate,
     taps_in,
@@ -24,6 +24,8 @@
     ln_shift,
     w_out,
     out,
+    tokens,
+    norm_gain,
     taps,
     weights,
     gathered,
@@ -55,7 +57,7 @@
     layers, depth, cols = w_value.shape
     kernel = taps_in.shape[0]
     half = (kernel - 1) // 2
-    count = tokens.shape[0]
+    count = tokens_in.shape[0]
     rows = count // chunks
     width = cols * tp
     hops = n - 1
@@ -96,24 +98,27 @@
         return pltpu.make_async_copy(
             source.at[layer, :, pl.ds(q * qc, qc)],
             weights.at[m, pl.ds(aligned(sp * depth, 16), depth), :],
-            load_sem.at[m],
-        )
-
-    taps_load = pltpu.make_async_copy(taps_in, taps, load_sem.at[total])
-    for m in range(total):
-        own_load(m).start()
-    taps_load.start()
+            load_sem.at[0 if m < 2 else 1],
+        )
+
+    tokens_load = pltpu.make_async_copy(tokens_in, tokens, load_sem.at[2])
+    gain_load = pltpu.make_async_copy(gain_in, norm_gain, load_sem.at[3])
+    taps_load = pltpu.make_async_copy(taps_in, taps, load_sem.at[4])
+    own_load(0).start()
+    own_load(1).start()
+    tokens_load.start()
+    gain_load.start()
 
     def piece(block, m, quarter):
         return weights.at[m, pl.ds(aligned(block * depth + quarter * part, 16), part), :]
 
-    def z_copy(way, m, hop, block):
+    def z_copy(way, m, block):
         ref = piece(block, m, grp)
         return pltpu.make_async_remote_copy(
             src_ref=ref,
             dst_ref=ref,
-            send_sem=z_send.at[way, m, hop],
-            recv_sem=z_recv.at[way, m, hop],
+            send_sem=z_send.at[way],
+            recv_sem=z_recv.at[m, block - way],
             device_id={"sp": sp + 1 if way == 0 else sp - 1},
             device_id_type=MESH,
         )
@@ -123,8 +128,8 @@
         return pltpu.make_async_remote_copy(
             src_ref=ref,
             dst_ref=ref,
-            send_sem=y_send.at[m, block, off - 1],
-            recv_sem=y_recv.at[m, block, off - 1],
+            send_sem=y_send.at[off - 1],
+            recv_sem=y_recv.at[m, off - 1],
             device_id={"grp": (grp + off) % groups},
             device_id_type=MESH,
         )
@@ -138,11 +143,11 @@
         @pl.when(sp - (r + 1) >= 0)
         def _():
             block = sp - (r + 1)
-            z_copy(0, m, r, block).wait_recv()
+            z_copy(0, m, block).wait_recv()
 
             @pl.when(sp < n - 1)
             def _():
-                z_copy(0, m, r + 1, block).start()
+                z_copy(0, m, block).start()
 
             for off in range(1, groups):
                 y_copy(m, block, off, grp).start()
@@ -150,11 +155,11 @@
         @pl.when(sp + (r + 1) < n)
         def _():
             block = sp + (r + 1)
-            z_copy(1, m, r, block).wait_recv()
+            z_copy(1, m, block).wait_recv()
 
             @pl.when(sp > 0)
             def _():
-                z_copy(1, m, r + 1, block).start()
+                z_copy(1, m, block).start()
 
             for off in range(1, groups):
                 y_copy(m, block, off, grp).start()
@@ -163,71 +168,68 @@
 
         @pl.when(jnp.logical_and(r == last_up, jnp.logical_and(more, sp < n - 1)))
         def _():
-            z_copy(0, m + 1, 0, sp).start()
-            z_copy(0, m + 2, 0, sp).start()
+            z_copy(0, m + 1, sp).start()
+            z_copy(0, m + 2, sp).start()
 
         @pl.when(jnp.logical_and(r == last_down, jnp.logical_and(more, sp > 0)))
         def _():
-            z_copy(1, m + 1, 0, sp).start()
-            z_copy(1, m + 2, 0, sp).start()
+            z_copy(1, m + 1, sp).start()
+            z_copy(1, m + 2, sp).start()
 
 
     def weight_steps(low, high):
         lax.fori_loop(low, high, lambda k, c: (weight_step(k), c)[1], 0)
 
+    def landed(ref, sem):
+        pltpu.make_async_copy(ref, ref, sem).wait()
+
     def weight_wait(m):
-        def wait(block, c):
-            @pl.when(block != sp)
-            def _():
-                for off in range(1, groups):
-                    y_copy(m, block, off, (grp + groups - off) % groups).wait_recv()
-
-            return c
-
-        lax.fori_loop(0, n, wait, 0)
+        for off in range(1, groups):
+            landed(weights.at[m, pl.ds(0, hops * part), :], y_recv.at[m, off - 1])
 
     def chunk_rows(c):
         return pl.ds(aligned(c * rows, rows), rows)
 
+    def x_lanes(phase, source):
+        sub = phase % (1 + subs)
+        if sub == 0:
+            return pl.ds(aligned(source * cols, LANES), cols)
+        return pl.ds(aligned(source * cols + (sub - 1) * qc, LANES), qc)
+
     def x_copy(phase, c, source, slot, target):
         layer, sub = phase // (1 + subs), phase % (1 + subs)
-        if sub == 0:
-            lanes = pl.ds(aligned(source * cols, LANES), cols)
-        else:
-            lanes = pl.ds(aligned(source * cols + (sub - 1) * qc, LANES), qc)
-        ref = gathered.at[2 * layer + min(sub, 1), chunk_rows(c), lanes]
+        ref = gathered.at[2 * layer + min(sub, 1), chunk_rows(c), x_lanes(phase, source)]
         return pltpu.make_async_remote_copy(
             src_ref=ref,
             dst_ref=ref,
-            send_sem=x_send.at[phase, c, slot],
-            recv_sem=x_recv.at[phase, c, source],
+            send_sem=x_send,
+            recv_sem=x_recv.at[phase, c, slot],
             device_id={"tp": target},
             device_id_type=MESH,
         )
 
     def x_own(phase, c):
         for off in range(1, chips):
-            x_copy(phase, c, me, off - 1, ((chip + off) % chips) * 2 + core).start()
-        x_copy(phase, c, me, chips - 1, partner).start()
+            x_copy(phase, c, me, off, ((chip + off) % chips) * 2 + core).start()
+        x_copy(phase, c, me, 0, partner).start()
 
     def x_forward(phase, c):
         for off in range(1, chips):
-            source = ((chip + off) % chips) * 2 + core
-            x_copy(phase, c, source, 0, partner).wait_recv()
-            x_copy(phase, c, source, chips - 1 + off, partner).start()
+            source = ((chip + chips - off) % chips) * 2 + core
+            x_copy(phase, c, source, off, partner).wait_recv()
+            x_copy(phase, c, source, 0, partner).start()
 
     def x_wait(phase, c):
-        for off in range(chips):
-            source = ((chip + off) % chips) * 2 + 1 - core
-            x_copy(phase, c, source, 0, partner).wait_recv()
-
-    def s_copy(phase, c, source, slot, target):
+        ref = gathered.at[0, pl.ds(0, rows), pl.ds(0, chips * (cols if phase % (1 + subs) == 0 else qc))]
+        landed(ref, x_recv.at[phase, c, 0])
+
+    def s_copy(phase, c, source, target):
         ref = stats.at[phase, c, source]
         return pltpu.make_async_remote_copy(
             src_ref=ref,
             dst_ref=ref,
-            send_sem=s_send.at[phase, c, slot],
-            recv_sem=s_recv.at[phase, c, source],
+            send_sem=s_send,
+            recv_sem=s_recv.at[phase, c],
             device_id={"tp": target},
             device_id_type=MESH,
         )
@@ -235,11 +237,10 @@
     def s_share(phase, c, values):
         stats[phase, c, me] = values.T[:8]
         for off in range(1, tp):
-            s_copy(phase, c, me, off - 1, (me + off) % tp).start()
+            s_copy(phase, c, me, (me + off) % tp).start()
 
     def s_wait(phase, c):
-        for off in range(1, tp):
-            s_copy(phase, c, (me + off) % tp, 0, me).wait_recv()
+        landed(stats.at[phase, c, pl.ds(0, tp - 1)], s_recv.at[phase, c])
 
     def s_total(phase, c):
         total = stats[phase, c, 0]
@@ -251,12 +252,16 @@
         block = jnp.concatenate(rows_of_8, axis=0)
         return jnp.concatenate([block] * (LANES // block.shape[0]), axis=0).T
 
-    def n_copy(which, source, slot, target):
+    def n_load(which):
+        source = (ln_gain, ln_shift)[which]
+        return pltpu.make_async_copy(source, norms.at[which, me], load_sem.at[5])
+
+    def n_copy(which, target):
         return pltpu.make_async_remote_copy(
             src_ref=(ln_gain, ln_shift)[which],
-            dst_ref=norms.at[which, source],
-            send_sem=n_send.at[which, slot],
-            recv_sem=n_recv.at[which, source],
+            dst_ref=norms.at[which, me],
+            send_sem=n_send,
+            recv_sem=n_recv,
             device_id={"tp": target},
             device_id_type=MESH,
         )
@@ -270,7 +275,7 @@
         return pltpu.make_async_remote_copy(
             src_ref=glu.at[layer, pl.ds(source, HALO), lanes],
             dst_ref=glu.at[layer, pl.ds(target, HALO), lanes],
-            send_sem=h_send.at[layer, q, way],
+            send_sem=h_send.at[way],
             recv_sem=h_recv.at[layer, q, way],
             device_id={"sp": device},
             device_id_type=MESH,
@@ -305,8 +310,7 @@
         def _():
             glu[layer, pl.ds(HALO + count, HALO), :] = jnp.zeros((HALO, cols), bf16)
 
-    for m in range(2):
-        own_load(m).wait()
+    landed(weights.at[pl.ds(0, 2), pl.ds(0, depth), :], load_sem.at[0])
     pl.semaphore_wait(
         barrier,
         tp - 1 + groups - 1 + (sp > 0).astype(jnp.int32) + (sp < n - 1).astype(jnp.int32),
@@ -315,21 +319,26 @@
 
         @pl.when(sp < n - 1)
         def _():
-            z_copy(0, m, 0, sp).start()
+            z_copy(0, m, sp).start()
 
         @pl.when(sp > 0)
         def _():
-            z_copy(1, m, 0, sp).start()
-
+            z_copy(1, m, sp).start()
+
+    for m in range(2, total):
+        own_load(m).start()
+    taps_load.start()
+    for which in range(2):
+        n_load(which).start()
+    tokens_load.wait()
+    gain_load.wait()
     loop(lambda c: share_stream(0, c, tokens[chunk_rows(c), :].astype(f32)))
     for which in range(2):
         for off in range(1, tp):
-            n_copy(which, me, off - 1, (me + off) % tp).start()
-    norms[0, me] = ln_gain[...]
-    norms[1, me] = ln_shift[...]
-    for m in range(2, total):
-        own_load(m).wait()
+            n_copy(which, (me + off) % tp).start()
+    landed(weights.at[pl.ds(2, total - 2), pl.ds(0, depth), :], load_sem.at[1])
     taps_load.wait()
+    landed(norms.at[:, 0], load_sem.at[5])
 
     done = [0]
 
@@ -398,7 +407,7 @@
 
         lax.fori_loop(0, rows // BLOCK * lane_blocks, block, 0)
 
-    def mixed(layer, q, steps, i):
+    def mixed(layer, q, forward, steps, i):
         c = inner_first(i)
 
         @pl.when(jnp.logical_and(c == 0, sp > 0))
@@ -423,6 +432,8 @@
             sums[chunk_rows(c), :] = both
         else:
             s_share(2 * layer + 1, c, both)
+        if forward is not None:
+            x_forward(forward, c)
         steps(i)
 
     def arrive(phase, steps, i):
@@ -437,8 +448,9 @@
         c = inner_first(i)
         phase = 2 * layer + 1
         x_forward(layer * (1 + subs) + subs, c)
-        x_wait(layer * (1 + subs) + subs, c)
         s_wait(phase, c)
+        for q in range(0 if layer else subs - 1, subs):
+            x_wait(layer * (1 + subs) + 1 + q, c)
         total = s_total(phase, c)
         mean = total[0:1]
         for q in range(1, subs):
@@ -462,17 +474,18 @@
                 act[chunk_rows(c), lanes] = (shaped + shaped * jnp.tanh(shaped)).astype(bf16)
         steps(i)
 
-    def close(layer, q, steps, i):
+    def close(layer, halves, steps, i):
         c = inner_first(i)
-        update = jnp.dot(
-            act[chunk_rows(c), :],
-            weights[layer * 3 * subs + 2 * subs + q],
-            preferred_element_type=f32,
-        )
-        source = tokens if layer == 0 else out
-        lanes = pl.ds(q * qc, qc)
-        out[chunk_rows(c), lanes] = (source[chunk_rows(c), lanes].astype(f32) + update).astype(bf16)
-        if q == subs - 1 and layer + 1 < layers:
+        for q in halves:
+            update = jnp.dot(
+                act[chunk_rows(c), :],
+                weights[layer * 3 * subs + 2 * subs + q],
+                preferred_element_type=f32,
+            )
+            source = tokens if layer == 0 else out
+            lanes = pl.ds(q * qc, qc)
+            out[chunk_rows(c), lanes] = (source[chunk_rows(c), lanes].astype(f32) + update).astype(bf16)
+        if layer + 1 < layers:
             share_stream(layer + 1, c, out[chunk_rows(c), :].astype(f32))
         steps(i)
 
@@ -482,76 +495,53 @@
     def part_of(steps):
         return steps * span // 6
 
+    marks = ((6, 7, 8, 9, 13, 14, 15, 16, 18, 20, 20, 22), (28, 28, 28, 30, 32, 33, 35, 36, 36, 36, 36, 36))
+
     for layer in range(layers):
         first = layer * 3 * subs
-        loop(functools.partial(arrive, layer * (1 + subs), share(done[0] + part_of(6))))
+        phase = layer * (1 + subs)
+        goals = iter([part_of(mark) for mark in marks[layer]])
+        loop(functools.partial(arrive, phase, share(next(goals))))
         if layer == 0:
-            for which in range(2):
-                for off in range(1, tp):
-                    n_copy(which, (me + off) % tp, 0, me).wait_recv()
+            landed(norms.at[:, pl.ds(0, tp - 1)], n_recv)
         for q in range(subs):
-            advance(need(first + 2 * q + 1) + part_of(2))
+            advance(max(need(first + 2 * q + 1), next(goals)))
             weight_wait(first + 2 * q)
             weight_wait(first + 2 * q + 1)
-            loop(functools.partial(gated, layer, q, share(done[0] + part_of(1))))
-            loop(functools.partial(mixed, layer, q, share(done[0] + part_of(1))))
-            if q < subs - 1:
-                loop(functools.partial(arrive, layer * (1 + subs) + 1 + q, share(done[0] + part_of(3))))
+            loop(functools.partial(gated, layer, q, share(next(goals))))
+            forward = phase + q if layer and q else None
+            loop(functools.partial(mixed, layer, q, forward, share(next(goals))))
+            if q < subs - 1 and layer == 0:
+                loop(functools.partial(arrive, phase + 1 + q, share(next(goals))))
         last = first + 2 * subs
-        advance(need(last + subs - 1) + 0)
-        loop(functools.partial(activate, layer, share(done[0] + 0)))
-        advance(need(last + subs - 1) + part_of(2))
-        for q in range(subs):
-            weight_wait(last + q)
-            loop(functools.partial(close, layer, q, share(done[0])))
-    advance(total * hops)
-
-    def drain_weights(i, carry):
-        m, block = i // n, i % n
-
-        @pl.when(block <= sp)
-        def _():
-            @pl.when(sp < n - 1)
-            def _():
-                z_copy(0, m, sp - block, block).wait_send()
-
-        @pl.when(block >= sp)
-        def _():
-            @pl.when(sp > 0)
-            def _():
-                z_copy(1, m, block - sp, block).wait_send()
-
-        @pl.when(block != sp)
-        def _():
-            for off in range(1, groups):
-                y_copy(m, block, off, grp).wait_send()
-
-        return carry
-
-    lax.fori_loop(0, total * n, drain_weights, 0)
-
-    def drain_chunks(c, carry):
-        for slot in range(tp - 1):
-            for phase in range(layers * (1 + subs)):
-                x_copy(phase, c, me, slot, partner).wait_send()
-            for phase in range(2 * layers):
-                s_copy(phase, c, me, slot, partner).wait_send()
-        return carry
-
-    lax.fori_loop(0, chunks, drain_chunks, 0)
-    for which in range(2):
-        for slot in range(tp - 1):
-            n_copy(which, me, slot, partner).wait_send()
-    for layer in range(layers):
-        for q in range(subs):
-
-            @pl.when(sp < n - 1)
-            def _():
-                h_copy(layer, q, 0).wait_send()
-
-            @pl.when(sp > 0)
-            def _():
-                h_copy(layer, q, 1).wait_send()
+        advance(next(goals))
+        loop(functools.partial(activate, layer, share(next(goals))))
+        advance(max(need(last + subs - 1), next(goals)))
+        if layer + 1 < layers:
+            for q in range(subs):
+                weight_wait(last + q)
+            loop(functools.partial(close, layer, range(subs), share(next(goals))))
+        else:
+            for q in range(subs):
+                weight_wait(last + q)
+                loop(functools.partial(close, layer, (q,), share(next(goals))))
+
+    for place in range(n):
+
+        @pl.when(sp == place)
+        def _():
+            if place < n - 1:
+                landed(weights.at[:, pl.ds(0, (place + 1) * part), :], z_send.at[0])
+                landed(glu.at[:, pl.ds(0, HALO), :], h_send.at[0])
+            if place > 0:
+                landed(weights.at[:, pl.ds(0, (n - place) * part), :], z_send.at[1])
+                landed(glu.at[:, pl.ds(0, HALO), :], h_send.at[1])
+
+    for off in range(1, groups):
+        landed(weights.at[:, pl.ds(0, hops * part), :], y_send.at[off - 1])
+    landed(gathered.at[:, :, pl.ds(0, (tp - 1) * cols)], x_send)
+    landed(stats.at[:, :, pl.ds(0, tp - 1)], s_send)
+    landed(norms.at[:, pl.ds(0, tp - 1)], n_send)
 
 
 def solution(mesh):
@@ -566,14 +556,16 @@
         taps = jnp.transpose(taps, (1, 0, 2))
         rows = count // chunks
         vmem = pl.BlockSpec(memory_space=pltpu.VMEM)
-        hbm = pl.BlockSpec(memory_space=pl.ANY)
+        hbm = pl.BlockSpec(memory_space=pltpu.HBM)
         dma = pltpu.SemaphoreType.DMA
         return pl.pallas_call(
             functools.partial(body, (groups, n, tp, chunks, subs)),
-            out_shape=jax.ShapeDtypeStruct((count, cols), jnp.bfloat16),
-            in_specs=[vmem, vmem, hbm, hbm, hbm, vmem, vmem, hbm],
+            out_shape=pltpu.VMEM((count, cols), jnp.bfloat16),
+            in_specs=[hbm] * 8,
             out_specs=vmem,
             scratch_shapes=[
+                pltpu.VMEM((count, cols), jnp.bfloat16),
+                pltpu.VMEM(norm_gain.shape, jnp.float32),
                 pltpu.VMEM(taps.shape, jnp.float32),
                 pltpu.VMEM((pieces, depth * n, cols // subs), jnp.bfloat16),
                 pltpu.VMEM((2 * layers, count, cols * tp), jnp.bfloat16),
@@ -583,22 +575,22 @@
                 pltpu.VMEM((count, LANES), jnp.float32),
                 pltpu.VMEM((2 * layers, chunks, tp, 8, rows), jnp.float32),
                 pltpu.VMEM((2, tp, layers, cols), jnp.float32),
-                dma((pieces + 1,)),
-                dma((2, pieces, n - 1)),
-                dma((2, pieces, n - 1)),
-                dma((pieces, n, groups - 1)),
-                dma((pieces, n, groups - 1)),
-                dma((layers * (1 + subs), chunks, tp - 1)),
-                dma((layers * (1 + subs), chunks, tp)),
-                dma((2 * layers, chunks, tp - 1)),
-                dma((2 * layers, chunks, tp)),
+                dma((6,)),
+                dma((2,)),
+                dma((pieces, n - 1)),
+                dma((groups - 1,)),
+                dma((pieces, groups - 1)),
+                dma,
+                dma((layers * (1 + subs), chunks, tp // 2)),
+                dma,
+                dma((2 * layers, chunks)),
+                dma((2,)),
                 dma((layers, subs, 2)),
-                dma((layers, subs, 2)),
-                dma((2, tp - 1)),
-                dma((2, tp)),
+                dma,
+                dma,
             ],
             compiler_params=pltpu.CompilerParams(
-                collective_id=0, has_side_effects=True, vmem_limit_bytes=60 * 1024 * 1024
+                collective_id=0, has_side_effects=True, vmem_limit_bytes=56 * 1024 * 1024
             ),
         )(tokens, norm_gain, w_value, w_gate, taps, ln_gain, ln_shift, w_out)
 

time: 138 us -> 125 us (0.906)
  Pallas kernels: 136 us -> 124 us
    pallas_call x1, Pallas kernels: 136 us -> 124 us  [shards(): pl.pallas_call(functools.partial(body, (groups, n, tp, chunks, subs)), ou...]
where the time goes in v2:
time: 125 us
  Pallas kernels  124 us (99%)
    pallas_call x1, Pallas kernels, shards(): pl.pallas_call(functools.partial(body, (groups, n, tp, chunks, subs)), ou...  124 us

profile of v2, /device:TPU:1, one launch (start us, length us, event | category | flops | bytes accessed | tf_op | source)
XLA Modules:
  0.0 124.6 jit_solution(7984467939720081798)
XLA Ops:
  0.0 123.7 %shard_map.82 = bf16[768,512]{1,0:T(8,128)(2,1)S(1)} custom-call(bf16[768,512]{1,0:T(8,128)(2,1)} %tokens_in.1, f32[2,2048]{1,0:T(2,128)} %gain_in.1, bf16[2,512,512]{2,1,0:T(8,128)(2,1)} %w_value.1, bf16[2,512,512]{2,1,0:T(8,128)(2,1)} %w_gate.1, f32[31,2,512]{2,1,0:T(2,128)} %bitcast.1, f32[2,512]{1,0:T(2,128)} %ln_gain.1, f32[2,512]{1,0:T(2,128)} %ln_shift.1, ...), custom_call_target="tpu_custom_call" | custom-call | tf_op jit(solution)/shard_map/pallas_call | solution.py:561
  123.7 0.9 copy.10

commit v3 on v2

--- a/solution.py
+++ b/solution.py
@@ -134,48 +134,41 @@
             device_id_type=MESH,
         )
 
-    last_up = jnp.maximum(sp - 1, 0)
-    last_down = jnp.maximum(n - 2 - sp, 0)
-
-    def weight_step(k):
-        m, r, p = 2 * (k // span) + k % 2, (k % span) // 2, k % 2
-
-        @pl.when(sp - (r + 1) >= 0)
-        def _():
-            block = sp - (r + 1)
-            z_copy(0, m, block).wait_recv()
-
-            @pl.when(sp < n - 1)
+    steps_in_all = total * hops
+    below, above = sp, n - 1 - sp
+    early = (0 * above, 0 * below)
+
+    def receive(way, k):
+        m, r = 2 * (k // span) + k % 2, (k % span) // 2
+        sources = below if way == 0 else above
+        onward = above > 0 if way == 0 else below > 0
+
+        @pl.when(r < sources)
+        def _():
+            block = sp - (r + 1) if way == 0 else sp + (r + 1)
+            z_copy(way, m, block).wait_recv()
+
+            @pl.when(onward)
             def _():
-                z_copy(0, m, block).start()
+                z_copy(way, m, block).start()
 
             for off in range(1, groups):
                 y_copy(m, block, off, grp).start()
 
-        @pl.when(sp + (r + 1) < n)
-        def _():
-            block = sp + (r + 1)
-            z_copy(1, m, block).wait_recv()
-
-            @pl.when(sp > 0)
+        @pl.when(jnp.logical_and(jnp.logical_and(r == sources, onward), m + 2 < total))
+        def _():
+            z_copy(way, m + 2, sp).start()
+
+    def weight_prelude():
+        for way in range(2):
+            lax.fori_loop(0, early[way], lambda k, c: (receive(way, k), c)[1], 0)
+
+    def weight_step(k):
+        for way in range(2):
+
+            @pl.when(k + early[way] < steps_in_all)
             def _():
-                z_copy(1, m, block).start()
-
-            for off in range(1, groups):
-                y_copy(m, block, off, grp).start()
-
-        more = jnp.logical_and(p == 1, m + 2 < total)
-
-        @pl.when(jnp.logical_and(r == last_up, jnp.logical_and(more, sp < n - 1)))
-        def _():
-            z_copy(0, m + 1, sp).start()
-            z_copy(0, m + 2, sp).start()
-
-        @pl.when(jnp.logical_and(r == last_down, jnp.logical_and(more, sp > 0)))
-        def _():
-            z_copy(1, m + 1, sp).start()
-            z_copy(1, m + 2, sp).start()
-
+                receive(way, k + early[way])
 
     def weight_steps(low, high):
         lax.fori_loop(low, high, lambda k, c: (weight_step(k), c)[1], 0)
@@ -291,11 +284,14 @@
         square = jnp.sum(wide * wide, axis=1, keepdims=True)
         s_share(2 * layer, c, jnp.where(lane == 0, square, 0.0))
 
-    def loop(function):
-        lax.fori_loop(0, chunks, lambda i, c: (function(i), c)[1], 0)
+    def loop(function, low=0, high=chunks):
+        lax.fori_loop(low, high, lambda i, c: (function(i), c)[1], 0)
 
     def inner_first(i):
         return (1 + 2 * i) % chunks
+
+    def conv_order(layer, i):
+        return (1 + (1 if layer else 2) * i) % chunks
 
     def ends_first(i):
         return (2 * i) % chunks
@@ -340,6 +336,7 @@
     taps_load.wait()
     landed(norms.at[:, 0], load_sem.at[5])
 
+    weight_prelude()
     done = [0]
 
     def share(goal):
@@ -357,7 +354,7 @@
         weight_steps(low, high)
 
     def gated(layer, q, steps, i):
-        c = ends_first(i)
+        c = inner_first(i) if layer and q == 0 else ends_first(i)
         if q == 0:
             s_wait(2 * layer, c)
         scale = lax.rsqrt(columns([s_total(2 * layer, c)])[:, :1] / width + 1e-06)
@@ -377,7 +374,8 @@
         def _():
             h_copy(layer, q, 0).start()
 
-        steps(i)
+        if steps is not None:
+            steps(i)
 
     shift = HALO - half
     groups_of_8 = (kernel + shift + 7) // 8
@@ -408,7 +406,7 @@
         lax.fori_loop(0, rows // BLOCK * lane_blocks, block, 0)
 
     def mixed(layer, q, forward, steps, i):
-        c = inner_first(i)
+        c = conv_order(layer, i)
 
         @pl.when(jnp.logical_and(c == 0, sp > 0))
         def _():
@@ -438,14 +436,15 @@
 
     def arrive(phase, steps, i):
         c = i if phase == 0 else inner_first(i)
-        steps(i)
+        if steps is not None:
+            steps(i)
         x_forward(phase, c)
         x_wait(phase, c)
 
     sublane = lax.broadcasted_iota(jnp.int32, (8, rows), 0)
 
     def activate(layer, steps, i):
-        c = inner_first(i)
+        c = conv_order(layer, i)
         phase = 2 * layer + 1
         x_forward(layer * (1 + subs) + subs, c)
         s_wait(phase, c)
@@ -495,20 +494,31 @@
     def part_of(steps):
         return steps * span // 6
 
-    marks = ((6, 7, 8, 9, 13, 14, 15, 16, 18, 20, 20, 22), (28, 28, 28, 30, 32, 33, 35, 36, 36, 36, 36, 36))
+    marks = ((6, 8, 9, 10, 13, 14, 15, 17, 18, 20, 20, 22), (24, 26, 26, 27, 28, 29, 32, 33, 35, 36, 36, 36, 36, 36))
 
     for layer in range(layers):
         first = layer * 3 * subs
         phase = layer * (1 + subs)
         goals = iter([part_of(mark) for mark in marks[layer]])
-        loop(functools.partial(arrive, phase, share(next(goals))))
         if layer == 0:
+            loop(functools.partial(arrive, phase, share(next(goals))))
             landed(norms.at[:, pl.ds(0, tp - 1)], n_recv)
+        else:
+            for i in range(chunks - 1):
+                advance(next(goals))
+                arrive(phase, None, i)
         for q in range(subs):
             advance(max(need(first + 2 * q + 1), next(goals)))
             weight_wait(first + 2 * q)
             weight_wait(first + 2 * q + 1)
-            loop(functools.partial(gated, layer, q, share(next(goals))))
+            if layer and q == 0:
+                loop(functools.partial(gated, layer, q, None), 0, chunks - 1)
+                advance(next(goals))
+                arrive(phase, None, chunks - 1)
+                gated(layer, q, None, chunks - 1)
+                advance(next(goals))
+            else:
+                loop(functools.partial(gated, layer, q, share(next(goals))))
             forward = phase + q if layer and q else None
             loop(functools.partial(mixed, layer, q, forward, share(next(goals))))
             if q < subs - 1 and layer == 0:

time: 125 us -> 118 us (0.944)
  Pallas kernels: 124 us -> 117 us
    pallas_call x1, Pallas kernels: 124 us -> 117 us  [shards(): pl.pallas_call(functools.partial(body, (groups, n, tp, chunks, subs)), ou...]
where the time goes in v3:
time: 118 us
  Pallas kernels  117 us (99%)
    pallas_call x1, Pallas kernels, shards(): pl.pallas_call(functools.partial(body, (groups, n, tp, chunks, subs)), ou...  117 us

profile of v3, /device:TPU:1, one launch (start us, length us, event | category | flops | bytes accessed | tf_op | source)
XLA Modules:
  0.0 118.3 jit_solution(193222991845364844)
XLA Ops:
  0.0 117.4 %shard_map.82 = bf16[768,512]{1,0:T(8,128)(2,1)S(1)} custom-call(bf16[768,512]{1,0:T(8,128)(2,1)} %tokens_in.1, f32[2,2048]{1,0:T(2,128)} %gain_in.1, bf16[2,512,512]{2,1,0:T(8,128)(2,1)} %w_value.1, bf16[2,512,512]{2,1,0:T(8,128)(2,1)} %w_gate.1, f32[31,2,512]{2,1,0:T(2,128)} %bitcast.1, f32[2,512]{1,0:T(2,128)} %ln_gain.1, f32[2,512]{1,0:T(2,128)} %ln_shift.1, ...), custom_call_target="tpu_custom_call" | custom-call | tf_op jit(solution)/shard_map/pallas_call | solution.py:571
  117.4 0.9 copy.10

commit v4 on v3

--- a/solution.py
+++ b/solution.py
@@ -471,10 +471,11 @@
                 block = gathered[phase, chunk_rows(c), lanes].astype(f32)
                 shaped = (block * table[:, 4:5] + offset) * gain + moved
                 act[chunk_rows(c), lanes] = (shaped + shaped * jnp.tanh(shaped)).astype(bf16)
-        steps(i)
+        if steps is not None:
+            steps(i)
 
     def close(layer, halves, steps, i):
-        c = inner_first(i)
+        c = inner_first(i) if layer + 1 < layers else conv_order(layer, i)
         for q in halves:
             update = jnp.dot(
                 act[chunk_rows(c), :],
@@ -486,7 +487,7 @@
             out[chunk_rows(c), lanes] = (source[chunk_rows(c), lanes].astype(f32) + update).astype(bf16)
         if layer + 1 < layers:
             share_stream(layer + 1, c, out[chunk_rows(c), :].astype(f32))
-        steps(i)
+            steps(i)
 
     def need(m):
         return (m // 2 + 1) * span
@@ -494,7 +495,7 @@
     def part_of(steps):
         return steps * span // 6
 
-    marks = ((6, 8, 9, 10, 13, 14, 15, 17, 18, 20, 20, 22), (24, 26, 26, 27, 28, 29, 32, 33, 35, 36, 36, 36, 36, 36))
+    marks = ((6, 8, 9, 10, 13, 14, 15, 17, 18, 20, 20, 22), (24, 26, 26, 27, 28, 29, 32, 33, 35, 36, 36, 36))
 
     for layer in range(layers):
         first = layer * 3 * subs
@@ -525,16 +526,24 @@
                 loop(functools.partial(arrive, phase + 1 + q, share(next(goals))))
         last = first + 2 * subs
         advance(next(goals))
-        loop(functools.partial(activate, layer, share(next(goals))))
-        advance(max(need(last + subs - 1), next(goals)))
         if layer + 1 < layers:
+            loop(functools.partial(activate, layer, share(next(goals))))
+            advance(max(need(last + subs - 1), next(goals)))
             for q in range(subs):
                 weight_wait(last + q)
             loop(functools.partial(close, layer, range(subs), share(next(goals))))
         else:
-            for q in range(subs):
+            for i in range(chunks - 1):
+                activate(layer, None, i)
+                advance(next(goals))
+            advance(steps_in_all)
+            weight_wait(last)
+            loop(functools.partial(close, layer, (0,), None), 0, chunks - 1)
+            activate(layer, None, chunks - 1)
+            close(layer, (0,), None, chunks - 1)
+            for q in range(1, subs):
                 weight_wait(last + q)
-                loop(functools.partial(close, layer, (q,), share(next(goals))))
+                loop(functools.partial(close, layer, (q,), None))
 
     for place in range(n):
 

time: 118 us -> 118 us (level)
  no operation moved by 1% of the time
where the time goes in v4:
time: 118 us
  Pallas kernels  117 us (99%)
    pallas_call x1, Pallas kernels, shards(): pl.pallas_call(functools.partial(body, (groups, n, tp, chunks, subs)), ou...  117 us

profile of v4, /device:TPU:1, one launch (start us, length us, event | category | flops | bytes accessed | tf_op | source)
XLA Modules:
  0.0 118.1 jit_solution(1726489475312560646)
XLA Ops:
  0.0 117.2 %shard_map.82 = bf16[768,512]{1,0:T(8,128)(2,1)S(1)} custom-call(bf16[768,512]{1,0:T(8,128)(2,1)} %tokens_in.1, f32[2,2048]{1,0:T(2,128)} %gain_in.1, bf16[2,512,512]{2,1,0:T(8,128)(2,1)} %w_value.1, bf16[2,512,512]{2,1,0:T(8,128)(2,1)} %w_gate.1, f32[31,2,512]{2,1,0:T(2,128)} %bitcast.1, f32[2,512]{1,0:T(2,128)} %ln_gain.1, f32[2,512]{1,0:T(2,128)} %ln_shift.1, ...), custom_call_target="tpu_custom_call" | custom-call | tf_op jit(solution)/shard_map/pallas_call | solution.py:580
  117.3 0.9 copy.10
